TPU v7x, 32 devices: a whole 2x2x4 slice. The times are simulated.
32 devices in a mesh: ep: 8 (over z, x), tp: 4 (over y, core).
Axes of the slice: x: 2, y: 2, z: 4, core: 2. Of those that a mesh axis runs over, the one named last changes fastest.
Arguments:
- tokens_a: bfloat16 [1024, 2048], P('ep'), may hold values from -6 to 6
- gain_a: float32 [2048], replicated, may hold values from 0.1 to 1.9
- value_w: bfloat16 [2048, 2048], P(None, 'tp'), may hold values from -0.125 to 0.125
- gate_w: bfloat16 [2048, 2048], P(None, 'tp'), may hold values from -0.125 to 0.125
- kernel: float32 [31, 2048], P(None, 'tp')
- chan_gain: float32 [2048], P('tp'), may hold values from 0.1 to 1.9
- out_w: bfloat16 [2048, 2048], P('tp'), may hold values from -0.125 to 0.125
- tokens_b: bfloat16 [1536, 2048], P('ep'), may hold values from -6 to 6
- gain_b: float32 [2048], replicated, may hold values from 0.1 to 1.9
- routes: int32 [1536, 2], P('ep'), may hold values from 0 to 7, all different within a row; in each aligned block of 192 rows (0 to 191, 192 to 383, ...) at most 72 rows name the same one
- route_logits: float32 [1536, 2], P('ep'), may hold values from -6 to 6
- expert_gate: bfloat16 [8, 2048, 2816], P('ep', None, 'tp'), may hold values from -0.125 to 0.125
- expert_up: bfloat16 [8, 2048, 2816], P('ep', None, 'tp'), may hold values from -0.125 to 0.125
- expert_down: bfloat16 [8, 2816, 2048], P('ep', 'tp'), may hold values from -0.109375 to 0.109375
Outputs:
- conv_out: bfloat16 [2048, 1024], P('tp', 'ep')
- moe_out: bfloat16 [2048, 1536], P('tp', 'ep')
Inputs may be any that keep to these rules, and one draw needn't show every extreme that they name: `routes`: each row names 2 different experts; among the rows of one index of ep no expert is named by more than 72 rows, a bound that some block reaches.
All inputs are finite; a program needn't handle non-finite values.
Results may differ from a plain program's by a relative error of at most 0.018.
Values may be sent and summed in bfloat16 or wider, within the bound.
A program may use at most 64 MiB of HBM per device.

v0:
```python
import functools

import jax
import jax.numpy as jnp
from jax import lax
from jax.experimental import pallas as pl
from jax.experimental.pallas import tpu as pltpu
from jax.sharding import PartitionSpec as P

MESH = pl.DeviceIdType.MESH
F32 = jnp.float32
BF16 = jnp.bfloat16
HALO = 32


def mm(a, b):
    return jnp.dot(a, b, preferred_element_type=F32)


def mt(a, b):
    return lax.dot_general(a, b, (((1,), (1,)), ((), ())), preferred_element_type=F32)


def kernel_body(
    n, ny, cap, groups, channels,
    tokens_a_h, gain_a, value_h, gate_h, taps, chan_gain, out_h,
    tokens_b_h, gain_b, routes, logits, eg_h, eu_h, ed_h,
    conv_o, moe_o,
    tok_a, tok_b, val_w, gat_w, out_w, eg, eu, ed,
    send, xbuf, gacc, uacc, hid, down_s, down_r, down_m, pair, yrecv, ret_s, ret_r,
    pad, tail, halo, st_s, st_r, st_ys, st_yr, conv_s, conv_r, conv_m, conv_p, conv_y,
    loc, a2a_ss, a2a_rs, fw_ss, fw_rs, ya_ss, ya_rs, yf_ss, yf_rs,
    dp_ss, dp_rs, dy_ss, dy_rs, rt_ss, rt_rs, one_ss, one_rs,
    sy_ss, sy_rs, cp_ss, cp_rs, cy_ss, cy_rs,
):
    e = lax.axis_index("ep")
    t = lax.axis_index("tp")
    y = t // 2
    c = t % 2
    partner = (e, y * 2 + (1 - c))
    feats = xbuf.shape[3]
    rows = n * cap
    per = n // groups

    def ep_peer(d):
        return (lax.rem(e + d, n), t)

    def y_peer(m):
        return (e, lax.rem(y + m, ny) * 2 + c)

    def remote(src, dst, ss, rs, device):
        return pltpu.make_async_remote_copy(
            src_ref=src, dst_ref=dst, send_sem=ss, recv_sem=rs, device_id=device, device_id_type=MESH
        )

    pairs = [(tokens_b_h, tok_b), (tokens_a_h, tok_a), (value_h, val_w), (gate_h, gat_w),
             (eg_h.at[0], eg), (eu_h.at[0], eu), (out_h, out_w), (ed_h.at[0], ed)]
    local = [pltpu.make_async_copy(src, dst, loc.at[i]) for i, (src, dst) in enumerate(pairs)]
    for copy in local:
        copy.start()

    barrier = pltpu.get_barrier_semaphore()
    for d in range(1, n):
        pl.semaphore_signal(barrier, inc=1, device_id=ep_peer(d), device_id_type=MESH)
    pl.semaphore_signal(barrier, inc=1, device_id=partner, device_id_type=MESH)
    for m in range(1, ny):
        pl.semaphore_signal(barrier, inc=1, device_id=y_peer(m), device_id_type=MESH)

    count = tok_b.shape[0]
    rel = routes[...] - e
    rel = jnp.where(rel < 0, rel + n, rel).astype(F32)
    row = lax.broadcasted_iota(jnp.int32, (count, count), 0)
    col = lax.broadcasted_iota(jnp.int32, (count, count), 1)

    def upright(line):
        return jnp.sum(jnp.where(row == col, line, 0.0), axis=1, keepdims=True)

    rel0, rel1 = upright(rel[0:1]), upright(rel[1:2])
    expert = lax.broadcasted_iota(jnp.int32, (count, n), 1).astype(F32)
    is0, is1 = expert == rel0, expert == rel1
    named = (jnp.where(is0, 1.0, 0.0) + jnp.where(is1, 1.0, 0.0)).astype(BF16)
    before = mm(jnp.where(row > col, 1.0, 0.0).astype(BF16), named)
    slot0 = rel0 * cap + jnp.sum(jnp.where(is0, before, 0.0), axis=1, keepdims=True)
    slot1 = rel1 * cap + jnp.sum(jnp.where(is1, before, 0.0), axis=1, keepdims=True)
    across0 = jnp.sum(jnp.where(row == col, slot0, 0.0), axis=0, keepdims=True)
    across1 = jnp.sum(jnp.where(row == col, slot1, 0.0), axis=0, keepdims=True)
    ids = lax.broadcasted_iota(jnp.int32, (rows, count), 0).astype(F32)
    pick = jnp.where((ids == across0) | (ids == across1), 1.0, 0.0).astype(BF16)

    local[0].wait()
    whole = tok_b[...].astype(F32)
    scale = lax.rsqrt(jnp.mean(whole * whole, axis=1, keepdims=True) + 1e-06)
    own_cols = pl.ds(pl.multiple_of(t * feats, feats), feats)
    mine = (tok_b[:, own_cols].astype(F32) * scale * gain_b[:, own_cols]).astype(BF16)
    picked = mm(pick, mine).reshape(n, cap, feats).astype(BF16)
    send[...] = picked
    xbuf[t, 0] = picked[0]

    pl.semaphore_wait(barrier, n + ny - 1)
    a2a = {}
    for d in range(1, n):
        a2a[d] = remote(send.at[d], xbuf.at[t, d], a2a_ss.at[d], a2a_rs.at[d], ep_peer(d))
        a2a[d].start()

    forwards, crossings, onward = [], {}, []

    def arrive(upto):
        for g in range(len(forwards), min(upto, groups)):
            for d in range(max(1, g * per), (g + 1) * per):
                a2a[d].wait_recv()
            part = xbuf.at[t, pl.ds(g * per, per)]
            for m in range(1, ny):
                copy = remote(part, part, ya_ss.at[m, g], ya_rs.at[m, g], y_peer(m))
                copy.start()
                crossings[m, g] = copy
            copy = remote(part, part, fw_ss.at[g], fw_rs.at[g], partner)
            copy.start()
            forwards.append(copy)

    def hand_on(upto):
        for g in range(len(onward), min(upto, groups)):
            copies = []
            for m in range(1, ny):
                crossings[m, g].wait_recv()
                block = lax.rem(y + ny - m, ny) * 2 + c
                part = xbuf.at[block, pl.ds(g * per, per)]
                copy = remote(part, part, yf_ss.at[m, g], yf_rs.at[m, g], partner)
                copy.start()
                copies.append(copy)
            onward.append(copies)

    cut = max(1, groups // 2)
    spans = [(0, cut), (cut, groups)]

    def project(block, h, first=False):
        lo, hi = spans[h][0] * per, spans[h][1] * per
        x = xbuf[block, pl.ds(lo, hi - lo)].astype(F32).reshape((hi - lo) * cap, feats).astype(BF16)
        at = pl.ds(pl.multiple_of(block * feats, feats), feats)
        to = pl.ds(lo * cap, (hi - lo) * cap)
        if first:
            gacc[to, :] = mt(x, eg[:, at])
            uacc[to, :] = mt(x, eu[:, at])
        else:
            gacc[to, :] += mt(x, eg[:, at])
            uacc[to, :] += mt(x, eu[:, at])

    def out_cols(m, core):
        block = lax.rem(y + m, ny) * 2 + core
        return pl.ds(pl.multiple_of(block * feats, feats), feats)

    down_x, down_y, returns = {}, {}, []
    order = list(range(1, ny)) + [0]

    def down(h):
        lo, hi = spans[h][0] * per, spans[h][1] * per
        to = pl.ds(lo * cap, (hi - lo) * cap)
        at = pl.ds(lo, hi - lo)
        hid[to, :] = (jax.nn.silu(gacc[to, :]) * uacc[to, :]).astype(BF16)
        for m in order:
            down_s[m, at] = mm(hid[to, :], ed[:, out_cols(m, 1 - c)]).reshape(hi - lo, cap, feats).astype(BF16)
            copy = remote(down_s.at[m, at], down_r.at[m, at], dp_ss.at[m, h], dp_rs.at[m, h], partner)
            copy.start()
            down_x[m, h] = copy
            down_m[m, at] = mm(hid[to, :], ed[:, out_cols(m, c)]).reshape(hi - lo, cap, feats)

    def cross(h):
        for m in order[:-1]:
            down_x[m, h].wait_recv()
        for g in range(*spans[h]):
            at = pl.ds(g * per, per)
            for m in order[:-1]:
                pair[m, at] = (down_m[m, at] + down_r[m, at].astype(F32)).astype(BF16)
                copy = remote(pair.at[m, at], yrecv.at[m, at], dy_ss.at[m, g], dy_rs.at[m, g], y_peer(m))
                copy.start()
                down_y[m, g] = copy
        down_x[0, h].wait_recv()

    def give_back(first, last):
        for g in range(first, last):
            at = pl.ds(g * per, per)
            summed = down_m[0, at] + down_r[0, at].astype(F32)
            for m in range(1, ny):
                down_y[m, g].wait_recv()
                summed = summed + yrecv[m, at].astype(F32)
            ret_s[at] = summed.astype(BF16)
            for d in range(g * per, (g + 1) * per):
                if d == 0:
                    ret_r[0] = summed[0].astype(BF16)
                else:
                    copy = remote(ret_s.at[d], ret_r.at[d], rt_ss.at[d], rt_rs.at[d], ep_peer(n - d))
                    copy.start()
                    returns.append(copy)

    def block_of(m, core):
        return lax.rem(y + ny - m, ny) * 2 + core

    arrive(1)

    local[1].wait()
    whole = tok_a[...].astype(F32)
    scale = lax.rsqrt(jnp.mean(whole * whole, axis=1, keepdims=True) + 1e-06)
    normed = (whole * scale * gain_a[...]).astype(BF16)
    local[2].wait()
    value = mm(normed, val_w[...])
    local[3].wait()
    glu = (value * jax.nn.sigmoid(mm(normed, gat_w[...]))).astype(BF16)
    length = glu.shape[0]
    tail[...] = glu[length - HALO:]
    rim = remote(tail, halo, one_ss.at[0], one_rs.at[0], ep_peer(1))
    rim.start()
    pad[HALO:] = glu.astype(F32)

    arrive(3)
    hand_on(1)
    arrive(4)
    hand_on(2)

    rim.wait_recv()
    pad[:HALO] = jnp.where(e > 0, halo[...].astype(F32), 0.0)
    width = taps.shape[0]
    chunk = min(128, pad.shape[1])
    total = jnp.zeros((length, 1), F32)
    square = jnp.zeros((length, 1), F32)
    mixed = []
    for lane in range(0, pad.shape[1], chunk):
        acc = jnp.zeros((length, chunk), F32)
        for tap in range(width):
            at = HALO - width + 1 + tap
            acc = acc + taps[tap:tap + 1, lane:lane + chunk] * pad[at:at + length, lane:lane + chunk]
        total = total + jnp.sum(acc, axis=1, keepdims=True)
        square = square + jnp.sum(acc * acc, axis=1, keepdims=True)
        mixed.append(acc)
    mixed = jnp.concatenate(mixed, axis=1)
    lanes = lax.broadcasted_iota(jnp.int32, (length, 128), 1)
    stats = jnp.where(lanes < 4, total, square).T
    st_s[...] = stats[0:8]
    stat = remote(st_s, st_r, one_ss.at[1], one_rs.at[1], partner)
    stat.start()

    arrive(5)
    hand_on(3)
    local[4].wait()
    local[5].wait()
    project(t, 0, True)
    arrive(6)
    hand_on(4)
    arrive(max(cut, min(6, groups)))
    hand_on(cut)

    stat.wait_recv()
    st_ys[...] = st_s[...] + st_r[...]
    stat_y = []
    for m in range(1, ny):
        copy = remote(st_ys, st_yr.at[m], sy_ss.at[m], sy_rs.at[m], y_peer(m))
        copy.start()
        stat_y.append(copy)

    for m in range(1, ny):
        project(block_of(m, c), 0)
    for g in range(cut):
        forwards[g].wait_recv()
    project(block_of(0, 1 - c), 0)
    arrive(7)
    hand_on(5)
    for g in range(cut):
        for copy in onward[g]:
            copy.wait_recv()
    for m in range(1, ny):
        project(block_of(m, 1 - c), 0)
    arrive(groups)
    hand_on(6)
    local[7].wait()
    down(0)
    hand_on(7)
    cross(0)

    sums = st_ys[...]
    for m in range(1, ny):
        stat_y[m - 1].wait_recv()
        sums = sums + st_yr[m]
    back = jnp.concatenate([sums] * (length // 8), axis=0).T
    average = back[:, 0:1] / channels
    spread = back[:, 4:5] / channels - average * average
    act = jax.nn.silu((mixed - average) * lax.rsqrt(spread + 1e-05) * chan_gain[...]).astype(BF16)
    local[6].wait()
    hand_on(groups)

    conv_x = []
    for m in range(ny):
        conv_s[m] = mm(act, out_w[:, out_cols(m, 1 - c)]).astype(BF16)
        copy = remote(conv_s.at[m], conv_r.at[m], cp_ss.at[m], cp_rs.at[m], partner)
        copy.start()
        conv_x.append(copy)
        conv_m[m] = mm(act, out_w[:, out_cols(m, c)])

    project(t, 1, True)
    for m in range(1, ny):
        project(block_of(m, c), 1)
    for g in range(cut, groups):
        forwards[g].wait_recv()
    project(block_of(0, 1 - c), 1)
    for g in range(cut, groups):
        for copy in onward[g]:
            copy.wait_recv()
    for m in range(1, ny):
        project(block_of(m, 1 - c), 1)
    give_back(0, cut // 2)
    down(1)
    cross(1)
    give_back(cut // 2, cut)

    conv_cross = []
    for m in range(ny):
        conv_x[m].wait_recv()
        summed = conv_m[m] + conv_r[m].astype(F32)
        if m == 0:
            conv_m[0] = summed
        else:
            conv_p[m] = summed.astype(BF16)
            copy = remote(conv_p.at[m], conv_y.at[m], cy_ss.at[m], cy_rs.at[m], y_peer(m))
            copy.start()
            conv_cross.append(copy)
    give_back(cut, groups)

    result = conv_m[0]
    for m in range(1, ny):
        conv_cross[m - 1].wait_recv()
        result = result + conv_y[m].astype(F32)
    conv_o[...] = result.astype(BF16)

    logit = logits[...]
    top = jnp.max(logit, axis=0, keepdims=True)
    exps = jnp.exp(logit - top)
    weight = exps / jnp.sum(exps, axis=0, keepdims=True)
    weight0, weight1 = upright(weight[0:1]), upright(weight[1:2])
    slots = lax.broadcasted_iota(jnp.int32, (count, rows), 1).astype(F32)
    combine = jnp.where(slots == slot0, weight0, 0.0) + jnp.where(slots == slot1, weight1, 0.0)
    high = combine.astype(BF16)
    low = (combine - high.astype(F32)).astype(BF16)
    for copy in returns:
        copy.wait_recv()
    returned = ret_r[...].astype(F32).reshape(rows, feats).astype(BF16)
    moe_o[...] = (mm(high, returned) + mm(low, returned)).astype(BF16)

    sent = list(a2a.values()) + forwards + list(crossings.values()) + [rim, stat] + stat_y + conv_x
    sent += sum(onward, []) + conv_cross + list(down_x.values()) + list(down_y.values()) + returns
    for copy in sent:
        copy.wait_send()


def solution(mesh):
    n = mesh.shape["ep"]
    n_tp = mesh.shape["tp"]
    ny = n_tp // 2
    groups = min(n, 8)

    def body(tokens_a, gain_a, value_w, gate_w, kernel, chan_gain, out_w,
             tokens_b, gain_b, routes, logits, eg, eu, ed):
        len_a, model = tokens_a.shape
        len_b = tokens_b.shape[0]
        chans = value_w.shape[1]
        feats = model // n_tp
        hidden = eg.shape[2]
        cap = 3 * len_b * routes.shape[1] // (2 * n)
        cap = -(-cap // 8) * 8
        rows = n * cap
        dma = pltpu.SemaphoreType.DMA
        vmem = pltpu.VMEM
        blocks = (n, cap, feats)
        scratch = [
            vmem((len_a, model), BF16), vmem((len_b, model), BF16),
            vmem((model, chans), BF16), vmem((model, chans), BF16), vmem((chans, model), BF16),
            vmem((hidden, model), BF16), vmem((hidden, model), BF16), vmem((hidden, model), BF16),
            vmem(blocks, BF16), vmem((n_tp,) + blocks, BF16),
            vmem((rows, hidden), F32), vmem((rows, hidden), F32), vmem((rows, hidden), BF16),
            vmem((ny,) + blocks, BF16), vmem((ny,) + blocks, BF16), vmem((ny,) + blocks, F32),
            vmem((ny,) + blocks, BF16), vmem((ny,) + blocks, BF16),
            vmem(blocks, BF16), vmem(blocks, BF16),
            vmem((HALO + len_a, chans), F32), vmem((HALO, chans), BF16), vmem((HALO, chans), BF16),
            vmem((8, len_a), F32), vmem((8, len_a), F32), vmem((8, len_a), F32), vmem((ny, 8, len_a), F32),
            vmem((ny, len_a, feats), BF16), vmem((ny, len_a, feats), BF16), vmem((ny, len_a, feats), F32),
            vmem((ny, len_a, feats), BF16), vmem((ny, len_a, feats), BF16),
            dma((8,)), dma((n,)), dma((n,)), dma((groups,)), dma((groups,)),
            dma((ny, groups)), dma((ny, groups)), dma((ny, groups)), dma((ny, groups)),
            dma((ny, 2)), dma((ny, 2)), dma((ny, groups)), dma((ny, groups)), dma((n,)), dma((n,)),
            dma((2,)), dma((2,)),
            dma((ny,)), dma((ny,)), dma((ny,)), dma((ny,)), dma((ny,)), dma((ny,)),
        ]
        hbm = pl.BlockSpec(memory_space=pl.ANY)
        near = pl.BlockSpec(memory_space=vmem)
        conv, moe = pl.pallas_call(
            functools.partial(kernel_body, n, ny, cap, groups, chans * n_tp),
            out_shape=(
                jax.ShapeDtypeStruct((len_a, feats), BF16),
                jax.ShapeDtypeStruct((len_b, feats), BF16),
            ),
            in_specs=[hbm, near, hbm, hbm, near, near, hbm, hbm, near, near, near, hbm, hbm, hbm],
            out_specs=(near, near),
            scratch_shapes=scratch,
            compiler_params=pltpu.CompilerParams(
                collective_id=0, has_side_effects=True, vmem_limit_bytes=60 * 1024 * 1024
            ),
        )(tokens_a, gain_a[None, :], value_w, gate_w, kernel, chan_gain[None, :], out_w,
          tokens_b, gain_b[None, :], routes.T, logits.T, eg.swapaxes(1, 2), eu.swapaxes(1, 2), ed)
        return conv.T, moe.T

    return jax.shard_map(
        body,
        mesh=mesh,
        in_specs=(
            P("ep", None), P(), P(None, "tp"), P(None, "tp"), P(None, "tp"), P("tp"), P("tp", None),
            P("ep", None), P(), P("ep", None), P("ep", None),
            P("ep", None, "tp"), P("ep", None, "tp"), P("ep", "tp", None),
        ),
        out_specs=(P("tp", "ep"), P("tp", "ep")),
        check_vma=False,
    )
```

profile of v0, /device:TPU:0, one launch (start us, length us, event | category | flops | bytes accessed | tf_op | source)
XLA Modules:
  0.0 58.1 jit_solution(17220973890036782728)
XLA Ops:
  0.6 54.2 %shard_map.149 = (bf16[128,512]{1,0:T(8,128)(2,1)}, bf16[192,512]{1,0:T(8,128)(2,1)}) custom-call(bf16[128,2048]{1,0:T(8,128)(2,1)} %tokens_a_h.1, f32[1,2048]{1,0:T(1,128)} %bitcast.13, bf16[2048,512]{1,0:T(8,128)(2,1)} %value_h.1, bf16[2048,512]{1,0:T(8,128)(2,1)} %gate_h.1, f32[31,512]{1,0:T(8,128)} %taps.1, f32[1,512]{1,0:T(1,128)} %bitcast.15, ...), custom_call_target="tpu_custom_call" | custom-call | tf_op jit(solution)/shard_map/pallas_call | solution.py:391
  54.8 1.7 %copy.16 = bf16[512,128]{1,0:T(8,128)(2,1)} copy(bf16[512,128]{0,1:T(8,128)(2,1)} %bitcast.12) | data formatting | bytes 262144
  56.5 1.6 %copy.18 = bf16[512,192]{0,1:T(8,128)(2,1)} copy(bf16[512,192]{0,1:T(8,128)(2,1)} %bitcast.11) | data formatting | bytes 393216
where the time goes:
time: 58.3 us; the launch traced here: 58.1 us
  Pallas kernels  54.2 us (93%)
  local copies, waits for them, and re-layouts  3.28 us (6%)
  between operations  0.64 us (1%)
    pallas_call x1, Pallas kernels, body(): pl.pallas_call(functools.partial(kernel_body, n, ny, cap, groups, chans *...  54.2 us
    unnamed x2, local copies, waits for them, and re-layouts  3.28 us

commit v1 on v0

--- a/solution.py
+++ b/solution.py
@@ -391,18 +391,33 @@
         conv, moe = pl.pallas_call(
             functools.partial(kernel_body, n, ny, cap, groups, chans * n_tp),
             out_shape=(
-                jax.ShapeDtypeStruct((len_a, feats), BF16),
-                jax.ShapeDtypeStruct((len_b, feats), BF16),
+                vmem((len_a, feats), BF16),
+                vmem((len_b, feats), BF16),
             ),
             in_specs=[hbm, near, hbm, hbm, near, near, hbm, hbm, near, near, near, hbm, hbm, hbm],
             out_specs=(near, near),
             scratch_shapes=scratch,
             compiler_params=pltpu.CompilerParams(
-                collective_id=0, has_side_effects=True, vmem_limit_bytes=60 * 1024 * 1024
+                collective_id=0, has_side_effects=True, vmem_limit_bytes=62914560
             ),
         )(tokens_a, gain_a[None, :], value_w, gate_w, kernel, chan_gain[None, :], out_w,
           tokens_b, gain_b[None, :], routes.T, logits.T, eg.swapaxes(1, 2), eu.swapaxes(1, 2), ed)
-        return conv.T, moe.T
+
+        def finish(conv_i, moe_i, conv_f, moe_f):
+            conv_f[...] = conv_i[...].T
+            moe_f[...] = moe_i[...]
+
+        conv, moe = pl.pallas_call(
+            finish,
+            out_shape=(
+                jax.ShapeDtypeStruct((feats, len_a), BF16),
+                jax.ShapeDtypeStruct((len_b, feats), BF16),
+            ),
+            in_specs=[near, near],
+            out_specs=(near, near),
+            compiler_params=pltpu.CompilerParams(vmem_limit_bytes=4 * 1024 * 1024),
+        )(conv, moe)
+        return conv, moe.T
 
     return jax.shard_map(
         body,

time: 58.3 us -> 55 us (0.943)
  local copies, waits for them, and re-layouts: 3.28 us -> 0 us
    unnamed x2 -> x0, local copies, waits for them, and re-layouts: 3.28 us -> none
    pallas_call x0 -> x1, Pallas kernels: none -> 0.75 us  [body(): pl.pallas_call(finish, out_shape=(jax.ShapeDtypeStruct((feats, len_a), BF...]
    pallas_call x1, Pallas kernels: 54.2 us -> 53.4 us  [body(): pl.pallas_call(functools.partial(kernel_body, n, ny, cap, groups, chans *...]
where the time goes in v1:
time: 55 us; the launch traced here: 54.8 us
  Pallas kernels  54.2 us (99%)
  between operations  0.64 us (1%)
    pallas_call x1, Pallas kernels, body(): pl.pallas_call(functools.partial(kernel_body, n, ny, cap, groups, chans *...  53.4 us

profile of v1, /device:TPU:0, one launch (start us, length us, event | category | flops | bytes accessed | tf_op | source)
XLA Modules:
  0.0 54.8 jit_solution(11388469182634068664)
XLA Ops:
  0.6 53.4 %shard_map.149 = (bf16[128,512]{1,0:T(8,128)(2,1)S(1)}, bf16[192,512]{1,0:T(8,128)(2,1)S(1)}) custom-call(bf16[128,2048]{1,0:T(8,128)(2,1)} %tokens_a_h.1, f32[1,2048]{1,0:T(1,128)} %bitcast.10, bf16[2048,512]{1,0:T(8,128)(2,1)} %value_h.1, bf16[2048,512]{1,0:T(8,128)(2,1)} %gate_h.1, f32[31,512]{1,0:T(8,128)} %taps.1, f32[1,512]{1,0:T(1,128)} %bitcast.12, ...), custom_call_target="tpu_custom_call" | custom-call | tf_op jit(solution)/shard_map/pallas_call | solution.py:391
  54.1 0.8 %shard_map.150 = (bf16[512,128]{1,0:T(8,128)(2,1)}, bf16[192,512]{1,0:T(8,128)(2,1)}) custom-call(bf16[128,512]{1,0:T(8,128)(2,1)S(1)} %get-tuple-element.6.conv_i, bf16[192,512]{1,0:T(8,128)(2,1)S(1)} %get-tuple-element.7.moe_i), custom_call_target="tpu_custom_call" | custom-call | tf_op jit(solution)/shard_map/pallas_call | solution.py:410

commit v2 on v1

v2 whole, which is shorter than its diff:
```python
import functools

import jax
import jax.numpy as jnp
from jax import lax
from jax.experimental import pallas as pl
from jax.experimental.pallas import tpu as pltpu
from jax.sharding import PartitionSpec as P

MESH = pl.DeviceIdType.MESH
F32 = jnp.float32
BF16 = jnp.bfloat16
HALO = 32


def mm(a, b):
    return jnp.dot(a, b, preferred_element_type=F32)


def mt(a, b):
    return lax.dot_general(a, b, (((1,), (1,)), ((), ())), preferred_element_type=F32)


def kernel_body(
    n, ny, cap, groups, near_groups, chunks, channels,
    tokens_a_h, gain_a_h, value_h, gate_h, taps_h, chan_gain_h, out_h,
    tokens_b_h, gain_b_h, routes_h, logits_h, eg_h, eu_h, ed_h,
    conv_o, moe_o,
    tok_a, tok_b, val_w, gat_w, out_w, eg, eu, ed, gain_a, gain_b, taps, chan_gain, routes, logits,
    send, nsend, xbuf, gacc, uacc, down_s, down_r, down_m, pair, yrecv, ret_s, ret_r,
    pad, tail, halo, st_s, st_r, st_ys, st_yr, conv_s, conv_r, conv_m, conv_p, conv_y,
    loc, a2a_ss, a2a_rs, nr_ss, nr_rs, fw_ss, fw_rs, ya_ss, ya_rs,
    dp_ss, dp_rs, dy_ss, dy_rs, rt_ss, rt_rs, one_ss, one_rs,
    sy_ss, sy_rs, cp_ss, cp_rs, cy_ss, cy_rs,
):
    e = lax.axis_index("ep")
    t = lax.axis_index("tp")
    y = t // 2
    c = t % 2
    partner = (e, y * 2 + (1 - c))
    feats = xbuf.shape[3]
    rows = n * cap
    per = n // groups
    near = near_groups * per

    def flip(v, d):
        bit = 1
        while bit <= d:
            if d & bit:
                v = v + bit - 2 * bit * lax.rem(v // bit, 2)
            bit *= 2
        return v

    def ep_peer(d):
        return (flip(e, d), t)

    def y_peer(m):
        return (e, lax.rem(y + m, ny) * 2 + c)

    def block_of(m, core):
        return lax.rem(y + ny - m, ny) * 2 + core

    def cols_of(block):
        return pl.ds(pl.multiple_of(block * feats, feats), feats)

    def remote(src, dst, ss, rs, device):
        return pltpu.make_async_remote_copy(
            src_ref=src, dst_ref=dst, send_sem=ss, recv_sem=rs, device_id=device, device_id_type=MESH
        )

    pairs = dict(
        routes=(routes_h, routes), tok_b=(tokens_b_h, tok_b), gain_b=(gain_b_h, gain_b),
        tok_a=(tokens_a_h, tok_a), gain_a=(gain_a_h, gain_a), val=(value_h, val_w), gat=(gate_h, gat_w),
        eg=(eg_h.at[0], eg), eu=(eu_h.at[0], eu), ed=(ed_h.at[0], ed), taps=(taps_h, taps),
        chan=(chan_gain_h, chan_gain), out=(out_h, out_w), logits=(logits_h, logits),
    )
    local = {
        name: pltpu.make_async_copy(src, dst, loc.at[i]) for i, (name, (src, dst)) in enumerate(pairs.items())
    }
    for name in ("routes", "tok_b", "gain_b"):
        local[name].start()

    barrier = pltpu.get_barrier_semaphore()
    for d in range(n - 1, 0, -1):
        pl.semaphore_signal(barrier, inc=1, device_id=ep_peer(d), device_id_type=MESH)
    pl.semaphore_signal(barrier, inc=1, device_id=partner, device_id_type=MESH)
    for m in range(1, ny):
        pl.semaphore_signal(barrier, inc=1, device_id=y_peer(m), device_id_type=MESH)
    for name in list(pairs)[3:]:
        local[name].start()

    count = tok_b.shape[0]
    row = lax.broadcasted_iota(jnp.int32, (count, count), 0)
    col = lax.broadcasted_iota(jnp.int32, (count, count), 1)

    def upright(line):
        return jnp.sum(jnp.where(row == col, line, 0.0), axis=1, keepdims=True)

    local["routes"].wait()
    rel = jnp.bitwise_xor(routes[...], e).astype(F32)
    rel0, rel1 = upright(rel[0:1]), upright(rel[1:2])
    expert = lax.broadcasted_iota(jnp.int32, (count, n), 1).astype(F32)
    is0, is1 = expert == rel0, expert == rel1
    named = (jnp.where(is0, 1.0, 0.0) + jnp.where(is1, 1.0, 0.0)).astype(BF16)
    before = mm(jnp.where(row > col, 1.0, 0.0).astype(BF16), named)
    slot0 = rel0 * cap + jnp.sum(jnp.where(is0, before, 0.0), axis=1, keepdims=True)
    slot1 = rel1 * cap + jnp.sum(jnp.where(is1, before, 0.0), axis=1, keepdims=True)
    across0 = jnp.sum(jnp.where(row == col, slot0, 0.0), axis=0, keepdims=True)
    across1 = jnp.sum(jnp.where(row == col, slot1, 0.0), axis=0, keepdims=True)

    def picker(lines):
        ids = lax.broadcasted_iota(jnp.int32, (lines, count), 0).astype(F32)
        return jnp.where((ids == across0) | (ids == across1), 1.0, 0.0).astype(BF16)

    pick = picker(rows)

    local["tok_b"].wait()
    local["gain_b"].wait()
    whole = tok_b[...].astype(F32)
    scale_b = lax.rsqrt(jnp.mean(whole * whole, axis=1, keepdims=True) + 1e-06)

    def normed_b(block):
        at = cols_of(block)
        return (tok_b[:, at].astype(F32) * scale_b * gain_b[:, at]).astype(BF16)

    picked = mm(pick, normed_b(t)).reshape(n, cap, feats).astype(BF16)
    send[...] = picked
    xbuf[t, 0] = picked[0]

    pl.semaphore_wait(barrier, n + ny - 1)
    a2a, nears, crossings, forwards = {}, {}, {}, {}
    k0, k1, k2, k3 = chunks

    def dispatch(k):
        for d in range(max(1, k[0] * per), k[1] * per):
            a2a[d] = remote(send.at[d], xbuf.at[t, d], a2a_ss.at[d], a2a_rs.at[d], ep_peer(d))
            a2a[d].start()

    dispatch((0, near_groups))
    dispatch(k2)
    dispatch((near_groups, k1[1]))

    pick_near, pick_own = picker(near * cap), picker(cap)
    for m in range(1, ny):
        block = block_of(m, c)
        picked = mm(pick_near, normed_b(block)).reshape(near, cap, feats).astype(BF16)
        nsend[m] = picked
        xbuf[block, 0] = picked[0]
        for d in range(1, near):
            copy = remote(nsend.at[m, d], xbuf.at[block, d], nr_ss.at[m, d], nr_rs.at[m, d], ep_peer(d))
            copy.start()
            nears[m, d] = copy
    for m in range(ny):
        block = block_of(m, 1 - c)
        xbuf[block, 0] = mm(pick_own, normed_b(block)).astype(BF16)

    def span(g):
        return max(1, g * per), (g + 1) * per

    def forward(m, g):
        lo, hi = span(g)
        if lo < hi:
            part = xbuf.at[block_of(m, c), pl.ds(lo, hi - lo)]
            copy = remote(part, part, fw_ss.at[m, g], fw_rs.at[m, g], partner)
            copy.start()
            forwards[m, g] = copy

    def arrive(g):
        lo, hi = span(g)
        for d in range(lo, hi):
            a2a[d].wait_recv()
        if g >= near_groups:
            part = xbuf.at[t, pl.ds(lo, hi - lo)]
            for m in range(1, ny):
                copy = remote(part, part, ya_ss.at[m, g], ya_rs.at[m, g], y_peer(m))
                copy.start()
                crossings[m, g] = copy
        forward(0, g)

    def hand_on(g):
        for m in range(1, ny):
            if g >= near_groups:
                crossings[m, g].wait_recv()
            else:
                for d in range(*span(g)):
                    nears[m, d].wait_recv()
            forward(m, g)

    def project(k, block, first=False):
        lo, hi = k[0] * per, k[1] * per
        x = xbuf[block, pl.ds(lo, hi - lo)].astype(F32).reshape((hi - lo) * cap, feats).astype(BF16)
        at = cols_of(block)
        to = pl.ds(lo * cap, (hi - lo) * cap)
        if first:
            gacc[to, :] = mt(x, eg[:, at])
            uacc[to, :] = mt(x, eu[:, at])
        else:
            gacc[to, :] += mt(x, eg[:, at])
            uacc[to, :] += mt(x, eu[:, at])

    def forwarded(k, m):
        for g in range(*k):
            if (m, g) in forwards:
                forwards[m, g].wait_recv()

    def project_near(k):
        project(k, t, True)
        forwarded(k, 0)
        project(k, block_of(0, 1 - c))

    def project_own(k):
        for m in range(1, ny):
            project(k, block_of(m, c))

    def project_last(k):
        for m in range(1, ny):
            forwarded(k, m)
            project(k, block_of(m, 1 - c))

    def out_cols(m, core):
        return cols_of(lax.rem(y + m, ny) * 2 + core)

    down_x, down_y, returns = {}, {}, []
    order = list(range(1, ny)) + [0]

    def down(k):
        i = chunks.index(k)
        lo, hi = k[0] * per, k[1] * per
        to = pl.ds(lo * cap, (hi - lo) * cap)
        at = pl.ds(lo, hi - lo)
        hid = (jax.nn.silu(gacc[to, :]) * uacc[to, :]).astype(BF16)
        for m in order:
            down_s[m, at] = mm(hid, ed[:, out_cols(m, 1 - c)]).reshape(hi - lo, cap, feats).astype(BF16)
            copy = remote(down_s.at[m, at], down_r.at[m, at], dp_ss.at[m, i], dp_rs.at[m, i], partner)
            copy.start()
            down_x[m, i] = copy
            down_m[m, at] = mm(hid, ed[:, out_cols(m, c)]).reshape(hi - lo, cap, feats)

    def cross(k):
        i = chunks.index(k)
        for m in order[:-1]:
            down_x[m, i].wait_recv()
        for g in range(*k):
            at = pl.ds(g * per, per)
            for m in order[:-1]:
                pair[m, at] = (down_m[m, at] + down_r[m, at].astype(F32)).astype(BF16)
                copy = remote(pair.at[m, at], yrecv.at[m, at], dy_ss.at[m, g], dy_rs.at[m, g], y_peer(m))
                copy.start()
                down_y[m, g] = copy
        down_x[0, i].wait_recv()

    def give_back(*gs):
        for g in gs:
            at = pl.ds(g * per, per)
            summed = down_m[0, at] + down_r[0, at].astype(F32)
            for m in range(1, ny):
                down_y[m, g].wait_recv()
                summed = summed + yrecv[m, at].astype(F32)
            ret_s[at] = summed.astype(BF16)
            for d in range(g * per, (g + 1) * per):
                if d == 0:
                    ret_r[0] = summed[0].astype(BF16)
                else:
                    copy = remote(ret_s.at[d], ret_r.at[d], rt_ss.at[d], rt_rs.at[d], ep_peer(d))
                    copy.start()
                    returns.append(copy)

    local["tok_a"].wait()
    local["gain_a"].wait()
    whole = tok_a[...].astype(F32)
    scale = lax.rsqrt(jnp.mean(whole * whole, axis=1, keepdims=True) + 1e-06)
    normed = (whole * scale * gain_a[...]).astype(BF16)
    local["val"].wait()
    value = mm(normed, val_w[...])
    local["gat"].wait()
    glu = (value * jax.nn.sigmoid(mm(normed, gat_w[...]))).astype(BF16)
    length = glu.shape[0]
    tail[...] = glu[length - HALO:]
    rim = remote(tail, halo, one_ss.at[0], one_rs.at[0], (lax.rem(e + 1, n), t))
    rim.start()
    dispatch(k3)
    pad[HALO:] = glu.astype(F32)

    local["eg"].wait()
    local["eu"].wait()
    if per > 1:
        arrive(0)
        hand_on(0)
    project_near(k0)
    project_own(k0)
    project_last(k0)
    local["ed"].wait()
    down(k0)
    arrive(6)
    arrive(1)
    hand_on(1)
    arrive(7)
    arrive(2)
    arrive(3)
    cross(k0)
    project_near(k2)

    local["taps"].wait()
    rim.wait_recv()
    pad[:HALO] = jnp.where(e > 0, halo[...].astype(F32), 0.0)
    width = taps.shape[0]
    chunk = min(128, pad.shape[1])
    total = jnp.zeros((length, 1), F32)
    square = jnp.zeros((length, 1), F32)
    mixed = []
    for lane in range(0, pad.shape[1], chunk):
        acc = jnp.zeros((length, chunk), F32)
        for tap in range(width):
            at = HALO - width + 1 + tap
            acc = acc + taps[tap:tap + 1, lane:lane + chunk] * pad[at:at + length, lane:lane + chunk]
        total = total + jnp.sum(acc, axis=1, keepdims=True)
        square = square + jnp.sum(acc * acc, axis=1, keepdims=True)
        mixed.append(acc)
    mixed = jnp.concatenate(mixed, axis=1)
    lanes = lax.broadcasted_iota(jnp.int32, (length, 128), 1)
    stats = jnp.where(lanes < 4, total, square).T
    st_s[...] = stats[0:8]
    stat = remote(st_s, st_r, one_ss.at[1], one_rs.at[1], partner)
    stat.start()

    hand_on(6)
    hand_on(7)
    project_own(k2)
    hand_on(2)
    project_last(k2)
    hand_on(3)
    down(k2)
    arrive(4)
    stat.wait_recv()
    st_ys[...] = st_s[...] + st_r[...]
    stat_y = []
    for m in range(1, ny):
        copy = remote(st_ys, st_yr.at[m], sy_ss.at[m], sy_rs.at[m], y_peer(m))
        copy.start()
        stat_y.append(copy)
    arrive(5)
    cross(k2)
    project_near(k1)
    project_own(k1)
    hand_on(4)
    project_last(k1)
    project_near(k3)
    hand_on(5)
    project_own(k3)
    give_back(6)
    project_last(k3)
    down(k3)
    give_back(7)
    cross(k3)
    down(k1)

    sums = st_ys[...]
    for m in range(1, ny):
        stat_y[m - 1].wait_recv()
        sums = sums + st_yr[m]
    local["chan"].wait()
    local["out"].wait()
    back = jnp.concatenate([sums] * (length // 8), axis=0).T
    average = back[:, 0:1] / channels
    spread = back[:, 4:5] / channels - average * average
    act = jax.nn.silu((mixed - average) * lax.rsqrt(spread + 1e-05) * chan_gain[...]).astype(BF16)

    conv_x = []
    for m in range(ny):
        conv_s[m] = mm(act, out_w[:, out_cols(m, 1 - c)]).astype(BF16)
        copy = remote(conv_s.at[m], conv_r.at[m], cp_ss.at[m], cp_rs.at[m], partner)
        copy.start()
        conv_x.append(copy)
        conv_m[m] = mm(act, out_w[:, out_cols(m, c)])

    cross(k1)
    give_back(4)

    conv_cross = []
    for m in range(ny):
        conv_x[m].wait_recv()
        summed = conv_m[m] + conv_r[m].astype(F32)
        if m == 0:
            conv_m[0] = summed
        else:
            conv_p[m] = summed.astype(BF16)
            copy = remote(conv_p.at[m], conv_y.at[m], cy_ss.at[m], cy_rs.at[m], y_peer(m))
            copy.start()
            conv_cross.append(copy)

    give_back(5)
    give_back(0, 1)

    local["logits"].wait()
    logit = logits[...]
    top = jnp.max(logit, axis=0, keepdims=True)
    exps = jnp.exp(logit - top)
    weight = exps / jnp.sum(exps, axis=0, keepdims=True)
    weight0, weight1 = upright(weight[0:1]), upright(weight[1:2])
    slots = lax.broadcasted_iota(jnp.int32, (count, rows), 1).astype(F32)
    combine = jnp.where(slots == slot0, weight0, 0.0) + jnp.where(slots == slot1, weight1, 0.0)
    high = combine.astype(BF16)
    low = (combine - high.astype(F32)).astype(BF16)
    give_back(2, 3)

    result = conv_m[0]
    for m in range(1, ny):
        conv_cross[m - 1].wait_recv()
        result = result + conv_y[m].astype(F32)
    conv_o[...] = result.astype(BF16)

    for copy in returns:
        copy.wait_recv()
    returned = ret_r[...].astype(F32).reshape(rows, feats).astype(BF16)
    moe_o[...] = (mm(high, returned) + mm(low, returned)).astype(BF16)

    sent = list(a2a.values()) + list(nears.values()) + list(crossings.values()) + list(forwards.values())
    sent += [rim, stat] + stat_y + conv_x + conv_cross
    sent += list(down_x.values()) + list(down_y.values()) + returns
    for copy in sent:
        copy.wait_send()


def solution(mesh):
    n = mesh.shape["ep"]
    n_tp = mesh.shape["tp"]
    ny = n_tp // 2
    groups = 8
    if n % groups or n & (n - 1):
        raise ValueError("ep size")
    near_groups = 2 if n == groups else 1
    chunks = [(0, 1), (1, 4), (6, 8), (4, 6)]

    def body(tokens_a, gain_a, value_w, gate_w, kernel, chan_gain, out_w,
             tokens_b, gain_b, routes, logits, eg, eu, ed):
        len_a, model = tokens_a.shape
        len_b = tokens_b.shape[0]
        chans = value_w.shape[1]
        feats = model // n_tp
        hidden = eg.shape[2]
        cap = 3 * len_b * routes.shape[1] // (2 * n)
        cap = -(-cap // 8) * 8
        rows = n * cap
        topk = routes.shape[1]
        near = near_groups * n // groups
        dma = pltpu.SemaphoreType.DMA
        vmem = pltpu.VMEM
        blocks = (n, cap, feats)
        scratch = [
            vmem((len_a, model), BF16), vmem((len_b, model), BF16),
            vmem((model, chans), BF16), vmem((model, chans), BF16), vmem((chans, model), BF16),
            vmem((hidden, model), BF16), vmem((hidden, model), BF16), vmem((hidden, model), BF16),
            vmem((1, model), F32), vmem((1, model), F32), vmem(kernel.shape, F32), vmem((1, chans), F32),
            vmem((topk, len_b), jnp.int32), vmem((topk, len_b), F32),
            vmem(blocks, BF16), vmem((ny, near, cap, feats), BF16), vmem((n_tp,) + blocks, BF16),
            vmem((rows, hidden), F32), vmem((rows, hidden), F32),
            vmem((ny,) + blocks, BF16), vmem((ny,) + blocks, BF16), vmem((ny,) + blocks, F32),
            vmem((ny,) + blocks, BF16), vmem((ny,) + blocks, BF16),
            vmem(blocks, BF16), vmem(blocks, BF16),
            vmem((HALO + len_a, chans), F32), vmem((HALO, chans), BF16), vmem((HALO, chans), BF16),
            vmem((8, len_a), F32), vmem((8, len_a), F32), vmem((8, len_a), F32), vmem((ny, 8, len_a), F32),
            vmem((ny, len_a, feats), BF16), vmem((ny, len_a, feats), BF16), vmem((ny, len_a, feats), F32),
            vmem((ny, len_a, feats), BF16), vmem((ny, len_a, feats), BF16),
            dma((14,)), dma((n,)), dma((n,)), dma((ny, near)), dma((ny, near)),
            dma((ny, groups)), dma((ny, groups)), dma((ny, groups)), dma((ny, groups)),
            dma((ny, 4)), dma((ny, 4)), dma((ny, groups)), dma((ny, groups)), dma((n,)), dma((n,)),
            dma((2,)), dma((2,)),
            dma((ny,)), dma((ny,)), dma((ny,)), dma((ny,)), dma((ny,)), dma((ny,)),
        ]
        hbm = pl.BlockSpec(memory_space=pl.ANY)
        here = pl.BlockSpec(memory_space=vmem)
        conv, moe = pl.pallas_call(
            functools.partial(kernel_body, n, ny, cap, groups, near_groups, chunks, chans * n_tp),
            out_shape=(
                vmem((len_a, feats), BF16),
                vmem((len_b, feats), BF16),
            ),
            in_specs=[hbm] * 14,
            out_specs=(here, here),
            scratch_shapes=scratch,
            compiler_params=pltpu.CompilerParams(
                collective_id=0, has_side_effects=True, vmem_limit_bytes=62914560
            ),
        )(tokens_a, gain_a[None, :], value_w, gate_w, kernel, chan_gain[None, :], out_w,
          tokens_b, gain_b[None, :], routes.T, logits.T, eg.swapaxes(1, 2), eu.swapaxes(1, 2), ed)

        def finish(conv_i, moe_i, conv_f, moe_f):
            conv_f[...] = conv_i[...].T
            moe_f[...] = moe_i[...]

        conv, moe = pl.pallas_call(
            finish,
            out_shape=(
                jax.ShapeDtypeStruct((feats, len_a), BF16),
                jax.ShapeDtypeStruct((len_b, feats), BF16),
            ),
            in_specs=[here, here],
            out_specs=(here, here),
            compiler_params=pltpu.CompilerParams(vmem_limit_bytes=4 * 1024 * 1024),
        )(conv, moe)
        return conv, moe.T

    return jax.shard_map(
        body,
        mesh=mesh,
        in_specs=(
            P("ep", None), P(), P(None, "tp"), P(None, "tp"), P(None, "tp"), P("tp"), P("tp", None),
            P("ep", None), P(), P("ep", None), P("ep", None),
            P("ep", None, "tp"), P("ep", None, "tp"), P("ep", "tp", None),
        ),
        out_specs=(P("tp", "ep"), P("tp", "ep")),
        check_vma=False,
    )
```

time: 55 us -> 50.3 us (0.915)
  Pallas kernels: 54.2 us -> 49.5 us
    pallas_call x1, Pallas kernels: 53.4 us -> 48.7 us  [body(): pl.pallas_call(functools.partial(kernel_body, n, ny, cap, groups, near_gr...]
where the time goes in v2:
time: 50.3 us; the launch traced here: 50.1 us
  Pallas kernels  49.5 us (98%)
  between operations  0.64 us (1%)
    pallas_call x1, Pallas kernels, body(): pl.pallas_call(functools.partial(kernel_body, n, ny, cap, groups, near_gr...  48.7 us

profile of v2, /device:TPU:0, one launch (start us, length us, event | category | flops | bytes accessed | tf_op | source)
XLA Modules:
  0.0 50.1 jit_solution(6061932007571248485)
XLA Ops:
  0.6 48.7 %shard_map.149 = (bf16[128,512]{1,0:T(8,128)(2,1)S(1)}, bf16[192,512]{1,0:T(8,128)(2,1)S(1)}) custom-call(bf16[128,2048]{1,0:T(8,128)(2,1)} %tokens_a_h.1, f32[1,2048]{1,0:T(1,128)} %bitcast.10, bf16[2048,512]{1,0:T(8,128)(2,1)} %value_h.1, bf16[2048,512]{1,0:T(8,128)(2,1)} %gate_h.1, f32[31,512]{1,0:T(8,128)} %taps_h.1, f32[1,512]{1,0:T(1,128)} %bitcast.12, ...), custom_call_target="tpu_custom_call" | custom-call | tf_op jit(solution)/shard_map/pallas_call | solution.py:472
  49.4 0.8 %shard_map.150 = (bf16[512,128]{1,0:T(8,128)(2,1)}, bf16[192,512]{1,0:T(8,128)(2,1)}) custom-call(bf16[128,512]{1,0:T(8,128)(2,1)S(1)} %get-tuple-element.6.conv_i, bf16[192,512]{1,0:T(8,128)(2,1)S(1)} %get-tuple-element.7.moe_i), custom_call_target="tpu_custom_call" | custom-call | tf_op jit(solution)/shard_map/pallas_call | solution.py:491

commit v3 on v2

--- a/solution.py
+++ b/solution.py
@@ -28,10 +28,8 @@
     conv_o, moe_o,
     tok_a, tok_b, val_w, gat_w, out_w, eg, eu, ed, gain_a, gain_b, taps, chan_gain, routes, logits,
     send, nsend, xbuf, gacc, uacc, down_s, down_r, down_m, pair, yrecv, ret_s, ret_r,
-    pad, tail, halo, st_s, st_r, st_ys, st_yr, conv_s, conv_r, conv_m, conv_p, conv_y,
-    loc, a2a_ss, a2a_rs, nr_ss, nr_rs, fw_ss, fw_rs, ya_ss, ya_rs,
-    dp_ss, dp_rs, dy_ss, dy_rs, rt_ss, rt_rs, one_ss, one_rs,
-    sy_ss, sy_rs, cp_ss, cp_rs, cy_ss, cy_rs,
+    pad, mix, tail, halo, st_s, st_r, st_ys, st_yr, conv_s, conv_r, conv_m, conv_p, conv_y,
+    loc, out_sem, a2a_rs, nr_rs, fw_rs, ya_rs, dp_rs, dy_rs, rt_rs, one_rs, sy_rs, cp_rs, cy_rs,
 ):
     e = lax.axis_index("ep")
     t = lax.axis_index("tp")
@@ -63,15 +61,15 @@
     def cols_of(block):
         return pl.ds(pl.multiple_of(block * feats, feats), feats)
 
-    def remote(src, dst, ss, rs, device):
+    def remote(src, dst, rs, device):
         return pltpu.make_async_remote_copy(
-            src_ref=src, dst_ref=dst, send_sem=ss, recv_sem=rs, device_id=device, device_id_type=MESH
+            src_ref=src, dst_ref=dst, send_sem=out_sem.at[0], recv_sem=rs, device_id=device, device_id_type=MESH
         )
 
     pairs = dict(
         routes=(routes_h, routes), tok_b=(tokens_b_h, tok_b), gain_b=(gain_b_h, gain_b),
         tok_a=(tokens_a_h, tok_a), gain_a=(gain_a_h, gain_a), val=(value_h, val_w), gat=(gate_h, gat_w),
-        eg=(eg_h.at[0], eg), eu=(eu_h.at[0], eu), ed=(ed_h.at[0], ed), taps=(taps_h, taps),
+        taps=(taps_h, taps), eg=(eg_h.at[0], eg), eu=(eu_h.at[0], eu), ed=(ed_h.at[0], ed),
         chan=(chan_gain_h, chan_gain), out=(out_h, out_w), logits=(logits_h, logits),
     )
     local = {
@@ -108,11 +106,9 @@
     across0 = jnp.sum(jnp.where(row == col, slot0, 0.0), axis=0, keepdims=True)
     across1 = jnp.sum(jnp.where(row == col, slot1, 0.0), axis=0, keepdims=True)
 
-    def picker(lines):
-        ids = lax.broadcasted_iota(jnp.int32, (lines, count), 0).astype(F32)
+    def picker(lo, hi):
+        ids = lax.broadcasted_iota(jnp.int32, ((hi - lo) * cap, count), 0).astype(F32) + lo * cap
         return jnp.where((ids == across0) | (ids == across1), 1.0, 0.0).astype(BF16)
-
-    pick = picker(rows)
 
     local["tok_b"].wait()
     local["gain_b"].wait()
@@ -123,33 +119,43 @@
         at = cols_of(block)
         return (tok_b[:, at].astype(F32) * scale_b * gain_b[:, at]).astype(BF16)
 
-    picked = mm(pick, normed_b(t)).reshape(n, cap, feats).astype(BF16)
-    send[...] = picked
-    xbuf[t, 0] = picked[0]
-
+    k0, k1, k2, k3 = chunks
+    own = normed_b(t)
+
+    def pick(lo, hi):
+        send[lo:hi] = mm(picker(lo, hi), own).reshape(hi - lo, cap, feats).astype(BF16)
+
+    pick(k2[0] * per, k2[1] * per)
     pl.semaphore_wait(barrier, n + ny - 1)
     a2a, nears, crossings, forwards = {}, {}, {}, {}
-    k0, k1, k2, k3 = chunks
 
     def dispatch(k):
         for d in range(max(1, k[0] * per), k[1] * per):
-            a2a[d] = remote(send.at[d], xbuf.at[t, d], a2a_ss.at[d], a2a_rs.at[d], ep_peer(d))
+            a2a[d] = remote(send.at[d], xbuf.at[t, d], a2a_rs.at[d], ep_peer(d))
             a2a[d].start()
 
-    dispatch((0, near_groups))
     dispatch(k2)
-    dispatch((near_groups, k1[1]))
-
-    pick_near, pick_own = picker(near * cap), picker(cap)
+    pick(0, k2[0] * per)
+    dispatch(k0)
+    dispatch(k1)
+    xbuf[t, 0] = send[0]
+
+    pick_near, pick_own = picker(0, near), picker(0, 1)
     for m in range(1, ny):
         block = block_of(m, c)
         picked = mm(pick_near, normed_b(block)).reshape(near, cap, feats).astype(BF16)
         nsend[m] = picked
         xbuf[block, 0] = picked[0]
-        for d in range(1, near):
-            copy = remote(nsend.at[m, d], xbuf.at[block, d], nr_ss.at[m, d], nr_rs.at[m, d], ep_peer(d))
-            copy.start()
-            nears[m, d] = copy
+
+    def second(k):
+        for m in range(1, ny):
+            for d in range(max(1, k[0] * per), k[1] * per):
+                to = xbuf.at[block_of(m, c), d]
+                copy = remote(nsend.at[m, d], to, nr_rs.at[m - 1, d], ep_peer(d))
+                copy.start()
+                nears[m, d] = copy
+
+    second(k0)
     for m in range(ny):
         block = block_of(m, 1 - c)
         xbuf[block, 0] = mm(pick_own, normed_b(block)).astype(BF16)
@@ -161,7 +167,7 @@
         lo, hi = span(g)
         if lo < hi:
             part = xbuf.at[block_of(m, c), pl.ds(lo, hi - lo)]
-            copy = remote(part, part, fw_ss.at[m, g], fw_rs.at[m, g], partner)
+            copy = remote(part, part, fw_rs.at[m, g], partner)
             copy.start()
             forwards[m, g] = copy
 
@@ -172,7 +178,7 @@
         if g >= near_groups:
             part = xbuf.at[t, pl.ds(lo, hi - lo)]
             for m in range(1, ny):
-                copy = remote(part, part, ya_ss.at[m, g], ya_rs.at[m, g], y_peer(m))
+                copy = remote(part, part, ya_rs.at[m - 1, g - near_groups], y_peer(m))
                 copy.start()
                 crossings[m, g] = copy
         forward(0, g)
@@ -203,10 +209,13 @@
             if (m, g) in forwards:
                 forwards[m, g].wait_recv()
 
+    def project_other(k):
+        forwarded(k, 0)
+        project(k, block_of(0, 1 - c))
+
     def project_near(k):
         project(k, t, True)
-        forwarded(k, 0)
-        project(k, block_of(0, 1 - c))
+        project_other(k)
 
     def project_own(k):
         for m in range(1, ny):
@@ -220,7 +229,7 @@
     def out_cols(m, core):
         return cols_of(lax.rem(y + m, ny) * 2 + core)
 
-    down_x, down_y, returns = {}, {}, []
+    down_x, down_y, returns = {}, {}, {}
     order = list(range(1, ny)) + [0]
 
     def down(k):
@@ -231,7 +240,7 @@
         hid = (jax.nn.silu(gacc[to, :]) * uacc[to, :]).astype(BF16)
         for m in order:
             down_s[m, at] = mm(hid, ed[:, out_cols(m, 1 - c)]).reshape(hi - lo, cap, feats).astype(BF16)
-            copy = remote(down_s.at[m, at], down_r.at[m, at], dp_ss.at[m, i], dp_rs.at[m, i], partner)
+            copy = remote(down_s.at[m, at], down_r.at[m, at], dp_rs.at[m, i], partner)
             copy.start()
             down_x[m, i] = copy
             down_m[m, at] = mm(hid, ed[:, out_cols(m, c)]).reshape(hi - lo, cap, feats)
@@ -244,7 +253,7 @@
             at = pl.ds(g * per, per)
             for m in order[:-1]:
                 pair[m, at] = (down_m[m, at] + down_r[m, at].astype(F32)).astype(BF16)
-                copy = remote(pair.at[m, at], yrecv.at[m, at], dy_ss.at[m, g], dy_rs.at[m, g], y_peer(m))
+                copy = remote(pair.at[m, at], yrecv.at[m, at], dy_rs.at[m - 1, g], y_peer(m))
                 copy.start()
                 down_y[m, g] = copy
         down_x[0, i].wait_recv()
@@ -261,9 +270,9 @@
                 if d == 0:
                     ret_r[0] = summed[0].astype(BF16)
                 else:
-                    copy = remote(ret_s.at[d], ret_r.at[d], rt_ss.at[d], rt_rs.at[d], ep_peer(d))
+                    copy = remote(ret_s.at[d], ret_r.at[d], rt_rs.at[d], ep_peer(d))
                     copy.start()
-                    returns.append(copy)
+                    returns[d] = copy
 
     local["tok_a"].wait()
     local["gain_a"].wait()
@@ -276,83 +285,96 @@
     glu = (value * jax.nn.sigmoid(mm(normed, gat_w[...]))).astype(BF16)
     length = glu.shape[0]
     tail[...] = glu[length - HALO:]
-    rim = remote(tail, halo, one_ss.at[0], one_rs.at[0], (lax.rem(e + 1, n), t))
+    rim = remote(tail, halo, one_rs.at[0], (lax.rem(e + 1, n), t))
     rim.start()
     dispatch(k3)
+    second(k1)
     pad[HALO:] = glu.astype(F32)
+
+    local["taps"].wait()
+    width = taps.shape[0]
+    chunk = min(128, pad.shape[1])
+
+    def convolve(first, last):
+        total = jnp.zeros((last - first, 1), F32)
+        square = jnp.zeros((last - first, 1), F32)
+        for lane in range(0, pad.shape[1], chunk):
+            acc = jnp.zeros((last - first, chunk), F32)
+            for tap in range(width):
+                at = HALO - width + 1 + tap
+                acc = acc + taps[tap:tap + 1, lane:lane + chunk] * pad[at + first:at + last, lane:lane + chunk]
+            total = total + jnp.sum(acc, axis=1, keepdims=True)
+            square = square + jnp.sum(acc * acc, axis=1, keepdims=True)
+            mix[first:last, lane:lane + chunk] = acc
+        return total, square
+
+    rest_total, rest_square = convolve(HALO, length)
 
     local["eg"].wait()
     local["eu"].wait()
     if per > 1:
         arrive(0)
         hand_on(0)
-    project_near(k0)
+    arrive(1)
+    project(k0, t, True)
+    hand_on(1)
     project_own(k0)
+    arrive(6)
+    project_other(k0)
     project_last(k0)
+    arrive(7)
     local["ed"].wait()
     down(k0)
-    arrive(6)
-    arrive(1)
-    hand_on(1)
-    arrive(7)
+    project(k2, t, True)
+    cross(k0)
     arrive(2)
     arrive(3)
-    cross(k0)
-    project_near(k2)
-
-    local["taps"].wait()
+    project_other(k2)
+    project(k1, t, True)
+
     rim.wait_recv()
     pad[:HALO] = jnp.where(e > 0, halo[...].astype(F32), 0.0)
-    width = taps.shape[0]
-    chunk = min(128, pad.shape[1])
-    total = jnp.zeros((length, 1), F32)
-    square = jnp.zeros((length, 1), F32)
-    mixed = []
-    for lane in range(0, pad.shape[1], chunk):
-        acc = jnp.zeros((length, chunk), F32)
-        for tap in range(width):
-            at = HALO - width + 1 + tap
-            acc = acc + taps[tap:tap + 1, lane:lane + chunk] * pad[at:at + length, lane:lane + chunk]
-        total = total + jnp.sum(acc, axis=1, keepdims=True)
-        square = square + jnp.sum(acc * acc, axis=1, keepdims=True)
-        mixed.append(acc)
-    mixed = jnp.concatenate(mixed, axis=1)
+    rim_total, rim_square = convolve(0, HALO)
+    total = jnp.concatenate([rim_total, rest_total], axis=0)
+    square = jnp.concatenate([rim_square, rest_square], axis=0)
     lanes = lax.broadcasted_iota(jnp.int32, (length, 128), 1)
     stats = jnp.where(lanes < 4, total, square).T
     st_s[...] = stats[0:8]
-    stat = remote(st_s, st_r, one_ss.at[1], one_rs.at[1], partner)
+    stat = remote(st_s, st_r, one_rs.at[1], partner)
     stat.start()
 
     hand_on(6)
     hand_on(7)
     project_own(k2)
-    hand_on(2)
-    project_last(k2)
-    hand_on(3)
-    down(k2)
-    arrive(4)
     stat.wait_recv()
     st_ys[...] = st_s[...] + st_r[...]
     stat_y = []
     for m in range(1, ny):
-        copy = remote(st_ys, st_yr.at[m], sy_ss.at[m], sy_rs.at[m], y_peer(m))
+        copy = remote(st_ys, st_yr.at[m], sy_rs.at[m - 1], y_peer(m))
         copy.start()
         stat_y.append(copy)
+    arrive(4)
+    project_last(k2)
     arrive(5)
+    hand_on(2)
+    hand_on(3)
+    down(k2)
+    project_other(k1)
     cross(k2)
-    project_near(k1)
+    give_back(0, 1)
     project_own(k1)
+    project_last(k1)
+    down(k1)
     hand_on(4)
-    project_last(k1)
-    project_near(k3)
+    project(k3, t, True)
+    project_other(k3)
+    cross(k1)
     hand_on(5)
     project_own(k3)
     give_back(6)
     project_last(k3)
     down(k3)
     give_back(7)
-    cross(k3)
-    down(k1)
 
     sums = st_ys[...]
     for m in range(1, ny):
@@ -363,18 +385,19 @@
     back = jnp.concatenate([sums] * (length // 8), axis=0).T
     average = back[:, 0:1] / channels
     spread = back[:, 4:5] / channels - average * average
-    act = jax.nn.silu((mixed - average) * lax.rsqrt(spread + 1e-05) * chan_gain[...]).astype(BF16)
+    act = jax.nn.silu((mix[...] - average) * lax.rsqrt(spread + 1e-05) * chan_gain[...]).astype(BF16)
 
     conv_x = []
     for m in range(ny):
         conv_s[m] = mm(act, out_w[:, out_cols(m, 1 - c)]).astype(BF16)
-        copy = remote(conv_s.at[m], conv_r.at[m], cp_ss.at[m], cp_rs.at[m], partner)
+        copy = remote(conv_s.at[m], conv_r.at[m], cp_rs.at[m], partner)
         copy.start()
         conv_x.append(copy)
         conv_m[m] = mm(act, out_w[:, out_cols(m, c)])
 
-    cross(k1)
-    give_back(4)
+    cross(k3)
+    give_back(2)
+    give_back(3)
 
     conv_cross = []
     for m in range(ny):
@@ -384,12 +407,9 @@
             conv_m[0] = summed
         else:
             conv_p[m] = summed.astype(BF16)
-            copy = remote(conv_p.at[m], conv_y.at[m], cy_ss.at[m], cy_rs.at[m], y_peer(m))
+            copy = remote(conv_p.at[m], conv_y.at[m], cy_rs.at[m - 1], y_peer(m))
             copy.start()
             conv_cross.append(copy)
-
-    give_back(5)
-    give_back(0, 1)
 
     local["logits"].wait()
     logit = logits[...]
@@ -397,11 +417,21 @@
     exps = jnp.exp(logit - top)
     weight = exps / jnp.sum(exps, axis=0, keepdims=True)
     weight0, weight1 = upright(weight[0:1]), upright(weight[1:2])
-    slots = lax.broadcasted_iota(jnp.int32, (count, rows), 1).astype(F32)
-    combine = jnp.where(slots == slot0, weight0, 0.0) + jnp.where(slots == slot1, weight1, 0.0)
-    high = combine.astype(BF16)
-    low = (combine - high.astype(F32)).astype(BF16)
-    give_back(2, 3)
+
+    def combined(k):
+        lo, hi = k[0] * per, k[1] * per
+        slots = lax.broadcasted_iota(jnp.int32, (count, (hi - lo) * cap), 1).astype(F32) + lo * cap
+        combine = jnp.where(slots == slot0, weight0, 0.0) + jnp.where(slots == slot1, weight1, 0.0)
+        high = combine.astype(BF16)
+        low = (combine - high.astype(F32)).astype(BF16)
+        for d in range(max(1, lo), hi):
+            returns[d].wait_recv()
+        came = ret_r[lo:hi].astype(F32).reshape((hi - lo) * cap, feats).astype(BF16)
+        return mm(high, came) + mm(low, came)
+
+    give_back(4)
+    moved = combined(k0)
+    give_back(5)
 
     result = conv_m[0]
     for m in range(1, ny):
@@ -409,14 +439,13 @@
         result = result + conv_y[m].astype(F32)
     conv_o[...] = result.astype(BF16)
 
-    for copy in returns:
-        copy.wait_recv()
-    returned = ret_r[...].astype(F32).reshape(rows, feats).astype(BF16)
-    moe_o[...] = (mm(high, returned) + mm(low, returned)).astype(BF16)
+    moved = moved + combined(k1)
+    moved = moved + combined(k2)
+    moe_o[...] = (moved + combined(k3)).astype(BF16)
 
     sent = list(a2a.values()) + list(nears.values()) + list(crossings.values()) + list(forwards.values())
     sent += [rim, stat] + stat_y + conv_x + conv_cross
-    sent += list(down_x.values()) + list(down_y.values()) + returns
+    sent += list(down_x.values()) + list(down_y.values()) + list(returns.values())
     for copy in sent:
         copy.wait_send()
 
@@ -428,8 +457,8 @@
     groups = 8
     if n % groups or n & (n - 1):
         raise ValueError("ep size")
-    near_groups = 2 if n == groups else 1
-    chunks = [(0, 1), (1, 4), (6, 8), (4, 6)]
+    near_groups = 4
+    chunks = [(0, 2), (2, 4), (6, 8), (4, 6)]
 
     def body(tokens_a, gain_a, value_w, gate_w, kernel, chan_gain, out_w,
              tokens_b, gain_b, routes, logits, eg, eu, ed):
@@ -457,15 +486,13 @@
             vmem((ny,) + blocks, BF16), vmem((ny,) + blocks, BF16), vmem((ny,) + blocks, F32),
             vmem((ny,) + blocks, BF16), vmem((ny,) + blocks, BF16),
             vmem(blocks, BF16), vmem(blocks, BF16),
-            vmem((HALO + len_a, chans), F32), vmem((HALO, chans), BF16), vmem((HALO, chans), BF16),
+            vmem((HALO + len_a, chans), F32), vmem((len_a, chans), F32), vmem((HALO, chans), BF16), vmem((HALO, chans), BF16),
             vmem((8, len_a), F32), vmem((8, len_a), F32), vmem((8, len_a), F32), vmem((ny, 8, len_a), F32),
             vmem((ny, len_a, feats), BF16), vmem((ny, len_a, feats), BF16), vmem((ny, len_a, feats), F32),
             vmem((ny, len_a, feats), BF16), vmem((ny, len_a, feats), BF16),
-            dma((14,)), dma((n,)), dma((n,)), dma((ny, near)), dma((ny, near)),
-            dma((ny, groups)), dma((ny, groups)), dma((ny, groups)), dma((ny, groups)),
-            dma((ny, 4)), dma((ny, 4)), dma((ny, groups)), dma((ny, groups)), dma((n,)), dma((n,)),
-            dma((2,)), dma((2,)),
-            dma((ny,)), dma((ny,)), dma((ny,)), dma((ny,)), dma((ny,)), dma((ny,)),
+            dma((14,)), dma((1,)), dma((n,)), dma((ny - 1, near)), dma((ny, groups)),
+            dma((ny - 1, groups - near_groups)), dma((ny, 4)), dma((ny - 1, groups)), dma((n,)),
+            dma((2,)), dma((ny - 1,)), dma((ny,)), dma((ny - 1,)),
         ]
         hbm = pl.BlockSpec(memory_space=pl.ANY)
         here = pl.BlockSpec(memory_space=vmem)

time: 50.3 us -> 45.3 us (0.901)
  Pallas kernels: 49.5 us -> 44.4 us
    pallas_call x1, Pallas kernels: 48.7 us -> 43.7 us  [body(): pl.pallas_call(functools.partial(kernel_body, n, ny, cap, groups, near_gr...]
where the time goes in v3:
time: 45.3 us; the launch traced here: 45.1 us
  Pallas kernels  44.4 us (98%)
  between operations  0.64 us (1%)
    pallas_call x1, Pallas kernels, body(): pl.pallas_call(functools.partial(kernel_body, n, ny, cap, groups, near_gr...  43.7 us

profile of v3, /device:TPU:0, one launch (start us, length us, event | category | flops | bytes accessed | tf_op | source)
XLA Modules:
  0.0 45.1 jit_solution(12692447217625159284)
XLA Ops:
  0.6 43.7 %shard_map.149 = (bf16[128,512]{1,0:T(8,128)(2,1)S(1)}, bf16[192,512]{1,0:T(8,128)(2,1)S(1)}) custom-call(bf16[128,2048]{1,0:T(8,128)(2,1)} %tokens_a_h.1, f32[1,2048]{1,0:T(1,128)} %bitcast.10, bf16[2048,512]{1,0:T(8,128)(2,1)} %value_h.1, bf16[2048,512]{1,0:T(8,128)(2,1)} %gate_h.1, f32[31,512]{1,0:T(8,128)} %taps_h.1, f32[1,512]{1,0:T(1,128)} %bitcast.12, ...), custom_call_target="tpu_custom_call" | custom-call | tf_op jit(solution)/shard_map/pallas_call | solution.py:499
  44.3 0.8 %shard_map.150 = (bf16[512,128]{1,0:T(8,128)(2,1)}, bf16[192,512]{1,0:T(8,128)(2,1)}) custom-call(bf16[128,512]{1,0:T(8,128)(2,1)S(1)} %get-tuple-element.6.conv_i, bf16[192,512]{1,0:T(8,128)(2,1)S(1)} %get-tuple-element.7.moe_i), custom_call_target="tpu_custom_call" | custom-call | tf_op jit(solution)/shard_map/pallas_call | solution.py:518

commit v4 on v3

--- a/solution.py
+++ b/solution.py
@@ -125,18 +125,20 @@
     def pick(lo, hi):
         send[lo:hi] = mm(picker(lo, hi), own).reshape(hi - lo, cap, feats).astype(BF16)
 
+    pick(0, k0[1] * per)
     pick(k2[0] * per, k2[1] * per)
     pl.semaphore_wait(barrier, n + ny - 1)
     a2a, nears, crossings, forwards = {}, {}, {}, {}
 
     def dispatch(k):
-        for d in range(max(1, k[0] * per), k[1] * per):
+        ds = list(range(max(1, k[0] * per), k[1] * per))
+        for d in ds[::-1] if k is k3 else ds:
             a2a[d] = remote(send.at[d], xbuf.at[t, d], a2a_rs.at[d], ep_peer(d))
             a2a[d].start()
 
+    dispatch(k0)
     dispatch(k2)
-    pick(0, k2[0] * per)
-    dispatch(k0)
+    pick(k0[1] * per, k2[0] * per)
     dispatch(k1)
     xbuf[t, 0] = send[0]
 
@@ -192,11 +194,12 @@
                     nears[m, d].wait_recv()
             forward(m, g)
 
-    def project(k, block, first=False):
+    def rows_of(k, block):
         lo, hi = k[0] * per, k[1] * per
-        x = xbuf[block, pl.ds(lo, hi - lo)].astype(F32).reshape((hi - lo) * cap, feats).astype(BF16)
-        at = cols_of(block)
-        to = pl.ds(lo * cap, (hi - lo) * cap)
+        return xbuf[block, pl.ds(lo, hi - lo)].astype(F32).reshape((hi - lo) * cap, feats).astype(BF16)
+
+    def accumulate(k, x, at, first):
+        to = pl.ds(k[0] * per * cap, (k[1] - k[0]) * per * cap)
         if first:
             gacc[to, :] = mt(x, eg[:, at])
             uacc[to, :] = mt(x, eu[:, at])
@@ -204,6 +207,9 @@
             gacc[to, :] += mt(x, eg[:, at])
             uacc[to, :] += mt(x, eu[:, at])
 
+    def project(k, block, first=False):
+        accumulate(k, rows_of(k, block), cols_of(block), first)
+
     def forwarded(k, m):
         for g in range(*k):
             if (m, g) in forwards:
@@ -213,9 +219,15 @@
         forwarded(k, 0)
         project(k, block_of(0, 1 - c))
 
-    def project_near(k):
-        project(k, t, True)
-        project_other(k)
+    def project_pair(k, m, first=False):
+        forwarded(k, m)
+        base = lax.rem(y + ny - m, ny) * 2
+        x = jnp.concatenate([rows_of(k, base), rows_of(k, base + 1)], axis=1)
+        accumulate(k, x, pl.ds(pl.multiple_of(base * feats, 2 * feats), 2 * feats), first)
+
+    def project_far(k):
+        for m in range(1, ny):
+            project_pair(k, m)
 
     def project_own(k):
         for m in range(1, ny):
@@ -238,28 +250,49 @@
         to = pl.ds(lo * cap, (hi - lo) * cap)
         at = pl.ds(lo, hi - lo)
         hid = (jax.nn.silu(gacc[to, :]) * uacc[to, :]).astype(BF16)
-        for m in order:
-            down_s[m, at] = mm(hid, ed[:, out_cols(m, 1 - c)]).reshape(hi - lo, cap, feats).astype(BF16)
+
+        def product(m, core):
+            return mm(hid, ed[:, out_cols(m, core)]).reshape(hi - lo, cap, feats)
+
+        def exchange(m):
             copy = remote(down_s.at[m, at], down_r.at[m, at], dp_rs.at[m, i], partner)
             copy.start()
             down_x[m, i] = copy
-            down_m[m, at] = mm(hid, ed[:, out_cols(m, c)]).reshape(hi - lo, cap, feats)
+
+        for m in order[:-1]:
+            down_s[m, at] = product(m, 1 - c).astype(BF16)
+            exchange(m)
+        for m in order[:-1]:
+            down_m[m, at] = product(m, c)
+        down_s[0, at] = product(0, 1 - c).astype(BF16)
+        down_m[0, at] = product(0, c)
+        exchange(0)
+
+    def cross_wait(k):
+        for m in order[:-1]:
+            down_x[m, chunks.index(k)].wait_recv()
+
+    def cross_one(g):
+        at = pl.ds(g * per, per)
+        for m in order[:-1]:
+            pair[m, at] = (down_m[m, at] + down_r[m, at].astype(F32)).astype(BF16)
+            copy = remote(pair.at[m, at], yrecv.at[m, at], dy_rs.at[m - 1, g], y_peer(m))
+            copy.start()
+            down_y[m, g] = copy
 
     def cross(k):
-        i = chunks.index(k)
-        for m in order[:-1]:
-            down_x[m, i].wait_recv()
-        for g in range(*k):
-            at = pl.ds(g * per, per)
-            for m in order[:-1]:
-                pair[m, at] = (down_m[m, at] + down_r[m, at].astype(F32)).astype(BF16)
-                copy = remote(pair.at[m, at], yrecv.at[m, at], dy_rs.at[m - 1, g], y_peer(m))
-                copy.start()
-                down_y[m, g] = copy
-        down_x[0, i].wait_recv()
+        cross_wait(k)
+        for g in reversed(range(*k)):
+            cross_one(g)
+
+    settled = []
 
     def give_back(*gs):
         for g in gs:
+            i = [k[0] <= g < k[1] for k in chunks].index(True)
+            if i not in settled:
+                down_x[0, i].wait_recv()
+                settled.append(i)
             at = pl.ds(g * per, per)
             summed = down_m[0, at] + down_r[0, at].astype(F32)
             for m in range(1, ny):
@@ -353,28 +386,26 @@
         copy = remote(st_ys, st_yr.at[m], sy_rs.at[m - 1], y_peer(m))
         copy.start()
         stat_y.append(copy)
+    arrive(5)
+    project_last(k2)
     arrive(4)
-    project_last(k2)
-    arrive(5)
     hand_on(2)
     hand_on(3)
     down(k2)
     project_other(k1)
     cross(k2)
-    give_back(0, 1)
-    project_own(k1)
-    project_last(k1)
+    give_back(1, 0)
+    project_far(k1)
     down(k1)
+    hand_on(5)
+    project_pair(k3, 0, True)
+    cross(k1)
     hand_on(4)
-    project(k3, t, True)
-    project_other(k3)
-    cross(k1)
-    hand_on(5)
     project_own(k3)
-    give_back(6)
+    give_back(7)
     project_last(k3)
     down(k3)
-    give_back(7)
+    give_back(6)
 
     sums = st_ys[...]
     for m in range(1, ny):
@@ -387,6 +418,8 @@
     spread = back[:, 4:5] / channels - average * average
     act = jax.nn.silu((mix[...] - average) * lax.rsqrt(spread + 1e-05) * chan_gain[...]).astype(BF16)
 
+    cross(k3)
+
     conv_x = []
     for m in range(ny):
         conv_s[m] = mm(act, out_w[:, out_cols(m, 1 - c)]).astype(BF16)
@@ -395,9 +428,8 @@
         conv_x.append(copy)
         conv_m[m] = mm(act, out_w[:, out_cols(m, c)])
 
-    cross(k3)
+    give_back(3)
     give_back(2)
-    give_back(3)
 
     conv_cross = []
     for m in range(ny):
@@ -429,9 +461,9 @@
         came = ret_r[lo:hi].astype(F32).reshape((hi - lo) * cap, feats).astype(BF16)
         return mm(high, came) + mm(low, came)
 
+    give_back(5)
+    moved = combined(k0)
     give_back(4)
-    moved = combined(k0)
-    give_back(5)
 
     result = conv_m[0]
     for m in range(1, ny):

time: 45.3 us -> 44.3 us (0.978)
  Pallas kernels: 44.4 us -> 43.5 us
    pallas_call x1, Pallas kernels: 43.7 us -> 42.7 us  [body(): pl.pallas_call(functools.partial(kernel_body, n, ny, cap, groups, near_gr...]
where the time goes in v4:
time: 44.3 us; the launch traced here: 44.1 us
  Pallas kernels  43.5 us (98%)
  between operations  0.64 us (1%)
    pallas_call x1, Pallas kernels, body(): pl.pallas_call(functools.partial(kernel_body, n, ny, cap, groups, near_gr...  42.7 us

profile of v4, /device:TPU:0, one launch (start us, length us, event | category | flops | bytes accessed | tf_op | source)
XLA Modules:
  0.0 44.1 jit_solution(2993482094907252929)
XLA Ops:
  0.6 42.7 %shard_map.149 = (bf16[128,512]{1,0:T(8,128)(2,1)S(1)}, bf16[192,512]{1,0:T(8,128)(2,1)S(1)}) custom-call(bf16[128,2048]{1,0:T(8,128)(2,1)} %tokens_a_h.1, f32[1,2048]{1,0:T(1,128)} %bitcast.10, bf16[2048,512]{1,0:T(8,128)(2,1)} %value_h.1, bf16[2048,512]{1,0:T(8,128)(2,1)} %gate_h.1, f32[31,512]{1,0:T(8,128)} %taps_h.1, f32[1,512]{1,0:T(1,128)} %bitcast.12, ...), custom_call_target="tpu_custom_call" | custom-call | tf_op jit(solution)/shard_map/pallas_call | solution.py:531
  43.4 0.8 %shard_map.150 = (bf16[512,128]{1,0:T(8,128)(2,1)}, bf16[192,512]{1,0:T(8,128)(2,1)}) custom-call(bf16[128,512]{1,0:T(8,128)(2,1)S(1)} %get-tuple-element.6.conv_i, bf16[192,512]{1,0:T(8,128)(2,1)S(1)} %get-tuple-element.7.moe_i), custom_call_target="tpu_custom_call" | custom-call | tf_op jit(solution)/shard_map/pallas_call | solution.py:550

commit v5 on v4

--- a/solution.py
+++ b/solution.py
@@ -359,11 +359,12 @@
     local["ed"].wait()
     down(k0)
     project(k2, t, True)
-    cross(k0)
     arrive(2)
     arrive(3)
+    project(k1, t, True)
     project_other(k2)
-    project(k1, t, True)
+    cross_wait(k0)
+    cross_one(1)
 
     rim.wait_recv()
     pad[:HALO] = jnp.where(e > 0, halo[...].astype(F32), 0.0)
@@ -394,7 +395,7 @@
     down(k2)
     project_other(k1)
     cross(k2)
-    give_back(1, 0)
+    give_back(1)
     project_far(k1)
     down(k1)
     hand_on(5)
@@ -419,6 +420,7 @@
     act = jax.nn.silu((mix[...] - average) * lax.rsqrt(spread + 1e-05) * chan_gain[...]).astype(BF16)
 
     cross(k3)
+    cross_one(0)
 
     conv_x = []
     for m in range(ny):
@@ -462,8 +464,11 @@
         return mm(high, came) + mm(low, came)
 
     give_back(5)
+    give_back(4)
+    give_back(0)
     moved = combined(k0)
-    give_back(4)
+    moved = moved + combined(k1)
+    moved = moved + combined(k2)
 
     result = conv_m[0]
     for m in range(1, ny):
@@ -471,9 +476,9 @@
         result = result + conv_y[m].astype(F32)
     conv_o[...] = result.astype(BF16)
 
-    moved = moved + combined(k1)
-    moved = moved + combined(k2)
-    moe_o[...] = (moved + combined(k3)).astype(BF16)
+    middle = (k3[0] + k3[1]) // 2
+    moved = moved + combined((middle, k3[1]))
+    moe_o[...] = (moved + combined((k3[0], middle))).astype(BF16)
 
     sent = list(a2a.values()) + list(nears.values()) + list(crossings.values()) + list(forwards.values())
     sent += [rim, stat] + stat_y + conv_x + conv_cross

time: 44.3 us -> 43.9 us (level)
  Pallas kernels: 43.5 us -> 43 us
    pallas_call x1, Pallas kernels: 42.7 us -> 42.3 us  [body(): pl.pallas_call(functools.partial(kernel_body, n, ny, cap, groups, near_gr...]
where the time goes in v5:
time: 43.9 us; the launch traced here: 43.7 us
  Pallas kernels  43 us (98%)
  between operations  0.64 us (1%)
    pallas_call x1, Pallas kernels, body(): pl.pallas_call(functools.partial(kernel_body, n, ny, cap, groups, near_gr...  42.3 us

profile of v5, /device:TPU:0, one launch (start us, length us, event | category | flops | bytes accessed | tf_op | source)
XLA Modules:
  0.0 43.7 jit_solution(8769669065098448656)
XLA Ops:
  0.6 42.3 %shard_map.149 = (bf16[128,512]{1,0:T(8,128)(2,1)S(1)}, bf16[192,512]{1,0:T(8,128)(2,1)S(1)}) custom-call(bf16[128,2048]{1,0:T(8,128)(2,1)} %tokens_a_h.1, f32[1,2048]{1,0:T(1,128)} %bitcast.10, bf16[2048,512]{1,0:T(8,128)(2,1)} %value_h.1, bf16[2048,512]{1,0:T(8,128)(2,1)} %gate_h.1, f32[31,512]{1,0:T(8,128)} %taps_h.1, f32[1,512]{1,0:T(1,128)} %bitcast.12, ...), custom_call_target="tpu_custom_call" | custom-call | tf_op jit(solution)/shard_map/pallas_call | solution.py:536
  42.9 0.8 %shard_map.150 = (bf16[512,128]{1,0:T(8,128)(2,1)}, bf16[192,512]{1,0:T(8,128)(2,1)}) custom-call(bf16[128,512]{1,0:T(8,128)(2,1)S(1)} %get-tuple-element.6.conv_i, bf16[192,512]{1,0:T(8,128)(2,1)S(1)} %get-tuple-element.7.moe_i), custom_call_target="tpu_custom_call" | custom-call | tf_op jit(solution)/shard_map/pallas_call | solution.py:555
